TPU v7x, 32 devices: a whole 2x2x4 slice. The times are simulated.
32 devices in a mesh: sp: 8 (over z, x), tp: 4 (over y, core).
Axes of the slice: x: 2, y: 2, z: 4, core: 2. Of those that a mesh axis runs over, the one named last changes fastest.
Arguments:
- residual: bfloat16 [4096, 4096], P('sp'), may hold values from -6 to 6
- queries: bfloat16 [4096, 1024], P('sp', 'tp'), may hold values from -6 to 6
- projected_key_rows: bfloat16 [4096, 1024], P('sp', 'tp'), may hold values from -6 to 6
- projected_value_rows: bfloat16 [4096, 2048], P('sp', 'tp'), may hold values from -6 to 6
- output_gate_logits: bfloat16 [4096, 2048], P('sp', 'tp'), may hold values from -6 to 6
- input_gate_logits: float32 [16, 4096], P('tp', 'sp'), may hold values from -8 to 120
- forget_gate_logits: float32 [16, 4096], P('tp', 'sp'), may hold values from 0 to 16
- extra_forget_logits: float32 [16, 4096], P('tp', 'sp'), may hold values from -0.7 to 0, as said below
- head_norm_gain: bfloat16 [2048], P('tp'), may hold values from 0.099609375 to 1.8984375
- output_projection_weight: bfloat16 [2048, 4096], P('tp'), may hold values from -0.125 to 0.125
- feedforward_norm_gain: bfloat16 [4096], replicated, may hold values from 0.099609375 to 1.8984375
- feedforward_gate_weight: bfloat16 [4096, 11264], P('sp', 'tp'), may hold values from -0.09375 to 0.09375
- up_projection_weight: bfloat16 [4096, 11264], P('sp', 'tp'), may hold values from -0.09375 to 0.09375
- down_projection_weight: bfloat16 [4096, 11264], P('sp', 'tp'), may hold values from -0.0546875 to 0.0546875
Outputs:
- layer_out: bfloat16 [4096, 4096], P(('sp', 'tp'))
Inputs may be any that keep to these rules, and one draw needn't show every extreme that they name: `extra_forget_logits`: each entry is 0 or the logarithm of a factor between one half and 0.8.
All inputs are finite; a program needn't handle non-finite values.
Results may differ from a plain program's by a relative error of at most 0.01.
Values may be sent and summed in bfloat16 or wider, within the bound.
A program may use at most 192 MiB of HBM per device.

v0:
```python
import functools
import jax
import jax.numpy as jnp
from jax import lax
from jax.experimental import pallas as pl
from jax.experimental.pallas import tpu as pltpu
from jax.sharding import PartitionSpec as P

MESH = pl.DeviceIdType.MESH
F32 = jnp.float32
BF16 = jnp.bfloat16
LANES = 128
QUERY_ROWS = 256
TOKEN_ROWS = 256
GATHER_CUTS = 2
EARLY_GROUPS = 3


class Plan:
    def __init__(self, mesh_shape, shapes):
        self.sp, self.tp = mesh_shape["sp"], mesh_shape["tp"]
        self.nz = next(n for n in range(1, self.sp + 1) if self.sp % n == 0 and n * n >= self.sp)
        self.nx = self.sp // self.nz
        self.nc = 2
        self.ny = self.tp // self.nc
        self.tok, self.d = shapes["residual"]
        self.own = self.tok // self.tp
        self.heads = shapes["gates"][0]
        self.qk = shapes["queries"][1] // self.heads
        self.vd = shapes["values"][1] // self.heads
        self.per = LANES // self.qk
        self.pairs = self.heads // self.per
        self.vw = shapes["values"][1]
        self.rows, self.ff = shapes["gate"]
        self.zc = self.nz // self.nc
        tiles = self.ff // LANES
        wide = -(-tiles // self.zc)
        starts = [min(i * wide, tiles - wide) for i in range(self.zc)]
        self.start = [s * LANES for s in starts]
        self.dup = [(i * wide - s) * LANES for i, s in enumerate(starts)]
        self.hid = wide * LANES
        self.nj = self.rows // LANES
        self.halves = 2
        self.sph = self.sp // self.halves
        self.cw = self.sph * LANES
        self.ns = self.nj * self.halves
        self.toks = self.nz * self.ny * self.own
        self.state_rows = self.pairs * LANES + -(-(self.pairs + 2 * self.heads) // 8) * 8
        self.wc = next(
            n for n in range(self.hid // LANES * LANES, 0, -LANES) if self.d % n == 0
        )
        self.cc = min(self.cw, self.wc)


def dotf(a, b, dims=(((1,), (0,)), ((), ())), precision=None):
    return lax.dot_general(a, b, dims, preferred_element_type=F32, precision=precision)


def split(a):
    high = a.astype(BF16)
    return high, (a - high.astype(F32)).astype(BF16)


def layer(p, *refs):
    (
        residual, queries, keys, values, out_gate, in_gate, forget, extra, head_gain, out_w,
        ff_gain, gate_w, up_w, down_w,
        out, gate_b, up_b, down_b,
        col, gated, xs, zs, carry, tokens, acc, slab, parts, yb, lb, rb, stream, cr, yr, res,
        s1_send, s1_recv, xf_send, xf_recv, pf_send, pf_recv,
        stx_send, stx_recv, stz_send, stz_recv, at_send, at_recv, ay_send, ay_recv,
        gz_right, gz_left, gz_recv, gy_send, gy_recv,
        ry_send, ry_recv, rr_send, rl_send, rl_recv, rr_recv, local,
    ) = refs
    nz, nx, ny, nc = p.nz, p.nx, p.ny, p.nc
    sp_i, tp_i = lax.axis_index("sp"), lax.axis_index("tp")
    z, x = sp_i // nx, lax.rem(sp_i, nx)
    y, c = tp_i // nc, lax.rem(tp_i, nc)
    other = 1 - c
    duty = c == 1 - z // p.zc

    def dev(z_, x_, y_, c_):
        return (z_ * nx + x_, y_ * nc + c_)

    def mod(a, e, n):
        return lax.rem(a + e, n)

    def remote(src, dst, send, recv, device):
        return pltpu.make_async_remote_copy(
            src_ref=src, dst_ref=dst, send_sem=send, recv_sem=recv,
            device_id=device, device_id_type=MESH,
        )

    barrier = pltpu.get_barrier_semaphore()
    friends = [dev(mod(z, e, nz), x, y, c) for e in range(1, nz)]
    friends += [dev(z, mod(x, e, nx), y, c) for e in range(1, nx)]
    friends += [dev(z, x, mod(y, e, ny), c) for e in range(1, ny)]
    friends += [dev(mod(z, e, nz), x, y, other) for e in range(nz)]
    for friend in friends:
        pl.semaphore_signal(barrier, inc=1, device_id=friend, device_id_type=MESH)
    pl.semaphore_wait(barrier, len(friends))

    mats = ((gate_w, gate_b), (up_w, up_b), (down_w, down_b))

    def jrows(j):
        return pl.ds(pl.multiple_of(j * LANES, LANES), LANES)

    def first_hop(m, j, i):
        src, dst = mats[m]
        return remote(
            src.at[jrows(j), pl.ds(p.start[i], p.hid)],
            dst.at[sp_i, jrows(j), :],
            s1_send.at[m, j, i], s1_recv.at[m, j, z],
            dev(c * p.zc + i, x, y, other),
        )

    def first_recv(m, j, zs_):
        src, dst = mats[m]
        view = dst.at[zs_ * nx + x, jrows(j), :]
        return remote(view, view, s1_send.at[m, j, 0], s1_recv.at[m, j, zs_], dev(z, x, y, other))

    def across(m, j, zs_, e):
        view = mats[m][1].at[zs_ * nx + x, jrows(j), :]
        return remote(
            view, view, xf_send.at[m, j, zs_, e - 1], xf_recv.at[m, j, zs_, e - 1],
            dev(z, mod(x, e, nx), y, c),
        )

    def across_recv(m, j, zs_, e):
        view = mats[m][1].at[zs_ * nx + mod(x, nx - e, nx), jrows(j), :]
        return remote(
            view, view, xf_send.at[m, j, zs_, e - 1], xf_recv.at[m, j, zs_, e - 1],
            dev(z, mod(x, e, nx), y, c),
        )

    def to_peer(m, j, sp_):
        view = mats[m][1].at[sp_, jrows(j), :]
        return remote(view, view, pf_send.at[m, j], pf_recv.at[m, j], dev(z, x, y, other))

    def peer_all(m, j):
        view = mats[m][1].at[:, jrows(j), :]
        return remote(view, view, pf_send.at[m, j], pf_recv.at[m, j], dev(z, x, y, other))

    def send_group(ms, j):
        for i in range(p.zc):
            for m in ms:
                first_hop(m, j, i).start()

    def each_z(fn):
        fn(z)
        for dist in range(1, nz):
            pl.when(z - dist >= 0)(functools.partial(fn, z - dist))
            pl.when(z + dist < nz)(functools.partial(fn, z + dist))

    def relay(ms, j):
        @pl.when(duty)
        def _():
            def one(zs_):
                for m in ms:
                    first_recv(m, j, zs_).wait_recv()
                    for e in range(1, nx):
                        across(m, j, zs_, e).start()
                    to_peer(m, j, zs_ * nx + x).start()

            each_z(one)

    def settle(ms, j):
        @pl.when(duty)
        def _():
            def one(zs_):
                for m in ms:
                    for e in range(1, nx):
                        across_recv(m, j, zs_, e).wait_recv()
                        to_peer(m, j, zs_ * nx + mod(x, nx - e, nx)).start()

            each_z(one)

        @pl.when(jnp.logical_not(duty))
        def _():
            for m in ms:
                peer_all(m, j).wait_recv()

    send_group((0, 1), 0)
    fetch_res = pltpu.make_async_copy(
        residual.at[pl.ds(pl.multiple_of(tp_i * p.own, p.own), p.own), :], res, local.at[2]
    )
    fetch_res.start()

    heads, per, pairs, tok = p.heads, p.per, p.pairs, p.tok
    fg = forget[...]
    lf = jnp.minimum(fg, 0.0) - jnp.log1p(jnp.exp(-jnp.abs(fg))) + extra[...]
    upper = (
        lax.broadcasted_iota(jnp.int32, (tok, tok), 0)
        <= lax.broadcasted_iota(jnp.int32, (tok, tok), 1)
    ).astype(F32)
    pad = jnp.zeros((-heads % 8, tok), F32)
    lf8 = jnp.concatenate([lf, pad], axis=0) if pad.shape[0] else lf
    cum_row = dotf(lf8, upper, precision=lax.Precision.HIGHEST)[:heads]
    ig = in_gate[...]
    pad = jnp.zeros((-2 * heads % 8, tok), F32)
    both = [cum_row, ig] + ([pad] if pad.shape[0] else [])
    col[...] = jnp.concatenate(both, axis=0).T
    bias_row = ig - cum_row
    base = pairs * LANES
    lane = lax.broadcasted_iota(jnp.int32, (1, LANES), 1) // p.qk
    subl = lax.broadcasted_iota(jnp.int32, (LANES, 1), 0) // p.qk

    def head_lanes(ref, h):
        pair = ref[:, h // per * LANES : (h // per + 1) * LANES]
        return jnp.where(lane == h % per, pair, jnp.zeros_like(pair))

    for pr in range(pairs):
        state = jnp.zeros((LANES, LANES), F32)
        norm = jnp.zeros((1, LANES), F32)
        for h in range(pr * per, (pr + 1) * per):
            total = cum_row[h : h + 1, tok - 1 : tok]
            log_w = total - col[:, h : h + 1] + col[:, heads + h : heads + h + 1]
            peak = jnp.max(log_w, axis=0, keepdims=True)
            weight = jnp.exp(log_w - peak)
            k_h = head_lanes(keys, h)
            high, low = split(values[:, h * p.vd : (h + 1) * p.vd].astype(F32) * weight)
            over = (((0,), (0,)), ((), ()))
            state += dotf(k_h, high, over) + dotf(k_h, low, over)
            norm += jnp.sum(k_h.astype(F32) * weight, axis=0, keepdims=True)
            row = base + pairs + h
            xs[x, row : row + 1, :] = jnp.broadcast_to(total, (1, LANES))
            row = base + pairs + heads + h
            xs[x, row : row + 1, :] = jnp.broadcast_to(peak, (1, LANES))
        xs[x, pr * LANES : (pr + 1) * LANES, :] = state
        xs[x, base + pr : base + pr + 1, :] = norm
    spare = p.state_rows - base - pairs - 2 * heads
    if spare:
        xs[x, p.state_rows - spare :, :] = jnp.zeros((spare, LANES), F32)

    def state_x(e):
        return remote(
            xs.at[x], xs.at[x], stx_send.at[e - 1], stx_recv.at[e - 1],
            dev(z, mod(x, e, nx), y, c),
        )

    def state_x_recv(e):
        view = xs.at[mod(x, nx - e, nx)]
        return remote(view, view, stx_send.at[e - 1], stx_recv.at[e - 1], dev(z, mod(x, e, nx), y, c))

    for e in range(1, nx):
        state_x(e).start()

    def join(target, later):
        lo = base + pairs
        tot_e, tot_l = target[lo : lo + heads, :], later[lo : lo + heads, :]
        pk_e = target[lo + heads : lo + 2 * heads, :]
        pk_l = later[lo + heads : lo + 2 * heads, :]
        pk = jnp.maximum(tot_l + pk_e, pk_l)
        w_e, w_l = jnp.exp(tot_l + pk_e - pk), jnp.exp(pk_l - pk)
        for pr in range(pairs):
            hs = [pr * per + i for i in range(per)]
            e_col = jnp.zeros((LANES, LANES), F32)
            l_col = jnp.zeros((LANES, LANES), F32)
            e_row = jnp.zeros((1, LANES), F32)
            l_row = jnp.zeros((1, LANES), F32)
            for i, h in enumerate(hs):
                e_col = jnp.where(subl == i, w_e[h : h + 1, :], e_col)
                l_col = jnp.where(subl == i, w_l[h : h + 1, :], l_col)
                e_row = jnp.where(lane == i, w_e[h : h + 1, :], e_row)
                l_row = jnp.where(lane == i, w_l[h : h + 1, :], l_row)
            blk = slice(pr * LANES, (pr + 1) * LANES)
            target[blk, :] = e_col * target[blk, :] + l_col * later[blk, :]
            row = slice(base + pr, base + pr + 1)
            target[row, :] = e_row * target[row, :] + l_row * later[row, :]
        target[lo : lo + heads, :] = tot_e + tot_l
        target[lo + heads : lo + 2 * heads, :] = pk

    def reset(target):
        target[...] = jnp.zeros((p.state_rows, LANES), F32)
        lo = base + pairs + heads
        target[lo : lo + heads, :] = jnp.full((heads, LANES), -1e30, F32)

    for e in range(1, nx):
        state_x_recv(e).wait_recv()
    mine = zs.at[z]
    reset(mine)
    for i in range(nx):
        join(mine, xs.at[i])

    def state_z(dist):
        return remote(
            zs.at[z], zs.at[z], stz_send.at[dist - 1], stz_recv.at[z],
            dev(lax.rem(z + dist, nz), x, y, c),
        )

    for dist in range(1, nz):
        pl.when(z + dist < nz)(lambda dist=dist: state_z(dist).start())
    for j in range(1, min(EARLY_GROUPS, p.nj)):
        send_group((0, 1), j)

    reset(carry)
    for i in range(nz - 1):

        @pl.when(i < z)
        def _(i=i):
            remote(zs.at[i], zs.at[i], stz_send.at[0], stz_recv.at[i], dev(z, x, y, other)).wait_recv()
            join(carry, zs.at[i])

    for i in range(nx - 1):
        pl.when(i < x)(lambda i=i: join(carry, xs.at[i]))

    lo = base + pairs
    total_in = carry[lo : lo + heads, :]
    peak_raw = carry[lo + heads : lo + 2 * heads, :]
    peak_all = jnp.maximum(peak_raw, total_in)
    scale_all = jnp.exp(peak_raw - peak_all)
    unit = p.qk ** (-0.5)
    qrows = min(QUERY_ROWS, tok)
    for h in range(heads):
        pr = h // per
        peak_in = peak_all[h : h + 1, 0:1]
        scale = scale_all[h : h + 1, :]
        st_high, st_low = split(carry[pr * LANES : (pr + 1) * LANES, :] * scale)
        norm_in = carry[base + pr : base + pr + 1, :] * scale
        k2 = keys[:, pr * LANES : (pr + 1) * LANES]
        v_h = values[:, h * p.vd : (h + 1) * p.vd]
        for r0 in range(0, tok, qrows):
            r1 = r0 + qrows
            q2 = queries[r0:r1, pr * LANES : (pr + 1) * LANES]
            q_h = jnp.where(lane == h % per, q2, jnp.zeros_like(q2))
            cum_c = col[r0:r1, h : h + 1]
            seen = (
                lax.broadcasted_iota(jnp.int32, (qrows, r1), 0) + r0
                >= lax.broadcasted_iota(jnp.int32, (qrows, r1), 1)
            )
            logs = jnp.where(seen, bias_row[h : h + 1, :r1], -jnp.inf) + cum_c
            inter = cum_c + peak_in
            peak_row = jnp.maximum(inter, jnp.max(logs, axis=1, keepdims=True))
            dots = dotf(q_h, k2[:r1], (((1,), (1,)), ((), ()))) * unit
            probs = dots * jnp.exp(logs - peak_row)
            inter_scale = jnp.exp(inter - peak_row) * unit
            high, low = split(probs)
            numer = dotf(high, v_h[:r1]) + dotf(low, v_h[:r1])
            numer += inter_scale * (dotf(q_h, st_high) + dotf(q_h, st_low))
            denom = jnp.sum(probs, axis=1, keepdims=True) + inter_scale * jnp.sum(
                q_h.astype(F32) * norm_in, axis=1, keepdims=True
            )
            cell = numer / jnp.maximum(jnp.abs(denom), jnp.exp(-peak_row))
            square = jnp.mean(cell * cell, axis=1, keepdims=True)
            span = slice(h * p.vd, (h + 1) * p.vd)
            gain = head_gain[:, span].astype(F32)
            gates = jax.nn.sigmoid(out_gate[r0:r1, span].astype(F32))
            gated[r0:r1, span] = (cell * lax.rsqrt(square + 1e-06) * gain * gates).astype(BF16)

    relay((0, 1), 0)

    pieces = p.d // p.wc

    def fetch_w(n):
        return pltpu.make_async_copy(
            out_w.at[:, pl.ds(n * p.wc, p.wc)],
            slab.at[n % 2, pl.ds(0, p.vw), pl.ds(0, p.wc)],
            local.at[n % 2],
        )

    fetch_w(0).start()
    for n in range(pieces):
        if n + 1 < pieces:
            fetch_w(n + 1).start()
        fetch_w(n).wait()
        for c0 in range(0, p.wc, p.cc):
            g0 = n * p.wc + c0
            w = slab[n % 2, : p.vw, c0 : c0 + p.cc]
            res_ = dotf(gated[...], w).astype(BF16)
            for b in range(p.tp):
                parts[g0 // p.cw, b // ny, b % ny, :, g0 % p.cw : g0 % p.cw + p.cc] = res_[
                    b * p.own : (b + 1) * p.own
                ]

    cols_used = p.d // p.cw

    def at_peer(yy):
        b = yy * nc + other
        return remote(
            parts.at[pl.ds(0, cols_used), b // ny, lax.rem(b, ny)],
            cr.at[:, yy], at_send.at[yy], at_recv.at[yy], dev(z, x, y, other),
        )

    for yy in range(ny):
        at_peer(yy).start()
    relay((0, 1), 1)

    def at_y(e):
        b = mod(y, e, ny) * nc + c
        return remote(
            parts.at[pl.ds(0, cols_used), b // ny, lax.rem(b, ny)],
            yr.at[:, e - 1], ay_send.at[e - 1], ay_recv.at[e - 1], dev(z, x, mod(y, e, ny), c),
        )

    for yy in range(ny):
        at_peer(yy).wait_recv()
    for e in range(1, ny):
        to = mod(y, e, ny)
        b = to * nc + c
        for n in range(cols_used):
            parts[n, b // ny, lax.rem(b, ny)] = (
                parts[n, b // ny, lax.rem(b, ny)].astype(F32) + cr[n, to].astype(F32)
            ).astype(BF16)
        at_y(e).start()
    fetch_res.wait()
    b = y * nc + c
    for n in range(cols_used):
        cols = slice(n * p.cw, (n + 1) * p.cw)
        stream[:, cols] = (
            res[:, cols].astype(F32)
            + parts[n, b // ny, lax.rem(b, ny)].astype(F32) + cr[n, y].astype(F32)
        )
    settle((0, 1), 0)
    for e in range(1, ny):
        at_y(e).wait_recv()
        for n in range(cols_used):
            cols = slice(n * p.cw, (n + 1) * p.cw)
            stream[:, cols] += yr[n, e - 1].astype(F32)
    cut = p.own // GATHER_CUTS
    for s in range(GATHER_CUTS):
        rows = slice(s * cut, (s + 1) * cut)
        part = stream[rows, :]
        square = jnp.mean(part * part, axis=1, keepdims=True)
        tokens[z, y, rows, :] = (
            part * lax.rsqrt(square + 1e-06) * ff_gain[...].astype(F32)
        ).astype(BF16)

    def block(zz, yy, s):
        return tokens.at[zz, yy, pl.ds(s * cut, cut), :]

    def go_right(zz, s):
        return remote(block(zz, y, s), block(zz, y, s), gz_right.at[zz, s], gz_recv.at[zz, s],
                      dev(z + 1, x, y, c))

    def go_left(zz, s):
        return remote(block(zz, y, s), block(zz, y, s), gz_left.at[zz, s], gz_recv.at[zz, s],
                      dev(z - 1, x, y, c))

    def go_y(zz, s, e):
        return remote(block(zz, y, s), block(zz, y, s), gy_send.at[zz, s, e - 1],
                      gy_recv.at[zz, s, e - 1], dev(z, x, mod(y, e, ny), c))

    def y_recv(zz, s, e):
        view = block(zz, mod(y, ny - e, ny), s)
        return remote(view, view, gy_send.at[zz, s, e - 1], gy_recv.at[zz, s, e - 1],
                      dev(z, x, mod(y, e, ny), c))

    for s in range(GATHER_CUTS):
        pl.when(z + 1 < nz)(lambda s=s: go_right(z, s).start())
        pl.when(z >= 1)(lambda s=s: go_left(z, s).start())
        for e in range(1, ny):
            go_y(z, s, e).start()
    for dist in range(1, nz):
        for s in range(GATHER_CUTS):

            @pl.when(z - dist >= 0)
            def _(dist=dist, s=s):
                go_right(z - dist, s).wait_recv()
                pl.when(z + 1 < nz)(lambda: go_right(z - dist, s).start())
                for e in range(1, ny):
                    go_y(z - dist, s, e).start()

            @pl.when(z + dist < nz)
            def _(dist=dist, s=s):
                go_left(z + dist, s).wait_recv()
                pl.when(z >= 1)(lambda: go_left(z + dist, s).start())
                for e in range(1, ny):
                    go_y(z + dist, s, e).start()

        if dist == 1:
            relay((0, 1), 2 % p.nj) if p.nj > 2 else None
    for j in range(min(EARLY_GROUPS, p.nj), p.nj):
        send_group((0, 1), j)
    for j in range(p.nj):
        send_group((2,), j)
    for j in range(1, min(3, p.nj)):
        settle((0, 1), j)
    for zz in range(nz):
        for s in range(GATHER_CUTS):
            for e in range(1, ny):
                y_recv(zz, s, e).wait_recv()
    for s in range(GATHER_CUTS):

        def sent(zz, s=s):
            pl.when((z + 1 < nz) & (zz <= z))(lambda: go_right(zz, s).wait_send())
            pl.when((z >= 1) & (zz >= z))(lambda: go_left(zz, s).wait_send())
            for e in range(1, ny):
                go_y(zz, s, e).wait_send()

        for zz in range(nz):
            sent(zz)

    trows = p.ny * p.own

    def load_slab(m, j):
        return [
            pltpu.make_async_copy(
                mats[m][1].at[s, jrows(j), :],
                slab.at[m, pl.ds(s * LANES, LANES), :],
                local.at[m],
            )
            for s in range(p.sp)
        ]

    def whole_slab(m):
        return pltpu.make_async_copy(slab.at[m], slab.at[m], local.at[m])

    for j in range(p.nj):
        if j >= 3:
            relay((0, 1), j)
            settle((0, 1), j)
        for m in range(2):
            for copy in load_slab(m, j):
                copy.start()
        for m in range(2):
            whole_slab(m).wait()

        @pl.loop(0, nz)
        def _(zz, j=j):
            lhs = jnp.concatenate(
                [
                    tokens[zz, :, :, s * p.rows + j * LANES : s * p.rows + (j + 1) * LANES].reshape(
                        trows, LANES
                    )
                    for s in range(p.sp)
                ],
                axis=1,
            )
            for m in range(2):
                more = dotf(lhs, slab[m])
                if j == 0:
                    acc[zz, m] = more
                else:
                    acc[zz, m] += more

    @pl.loop(0, nz)
    def _(zz):
        hidden = jax.nn.silu(acc[zz, 0]) * acc[zz, 1]
        if any(p.dup):
            seen_col = lax.broadcasted_iota(jnp.int32, (1, p.hid), 1)
            for i in range(p.zc):
                if p.dup[i]:
                    drop = (seen_col < p.dup[i]) & (lax.rem(z, p.zc) == i)
                    hidden = jnp.where(drop, 0.0, hidden)
        tokens[zz, :, :, : p.hid] = hidden.astype(BF16).reshape(ny, p.own, p.hid)

    def ry(n, e):
        return remote(
            parts.at[n, :, mod(y, e, ny)], yb.at[n, e - 1], ry_send.at[n, e - 1],
            ry_recv.at[n, e - 1], dev(z, x, mod(y, e, ny), c),
        )

    def rz_right(n, o):
        return remote(parts.at[n, o, y], lb.at[n, o - 1], rr_send.at[n, o], rl_recv.at[n, o],
                      dev(z + 1, x, y, c))

    def rz_left(n, o):
        return remote(parts.at[n, o, y], rb.at[n, o], rl_send.at[n, o], rr_recv.at[n, o],
                      dev(z - 1, x, y, c))

    for yy in range(ny):
        at_peer(yy).wait_send()
    for e in range(1, ny):
        at_y(e).wait_send()

    def add_stream(n, more):
        j, half = n // p.halves, lax.rem(n, p.halves)
        for q in range(p.sph):
            at = pl.multiple_of((half * p.sph + q) * p.rows + j * LANES, LANES)
            stream[:, pl.ds(at, LANES)] += 0.5 * more[:, q * LANES : (q + 1) * LANES]

    def load_down(n):
        j, half = n // p.halves, lax.rem(n, p.halves)
        return [
            pltpu.make_async_copy(
                down_b.at[half * p.sph + q, jrows(j), :],
                slab.at[0, pl.ds(q * LANES, LANES), :],
                local.at[0],
            )
            for q in range(p.sph)
        ]

    def step(i, _):
        @pl.when(i < p.ns)
        def _():
            j = i // p.halves

            @pl.when(lax.rem(i, p.halves) == 0)
            def _():
                relay((2,), j)
                settle((2,), j)

            for copy in load_down(i):
                copy.start()
            view = slab.at[0, pl.ds(0, p.sph * LANES), :]
            pltpu.make_async_copy(view, view, local.at[0]).wait()

            @pl.loop(0, nz)
            def _(zz):
                hid = tokens[zz, :, :, : p.hid].reshape(trows, p.hid)
                terms = dotf(hid, slab[0, : p.sph * LANES, :], (((1,), (1,)), ((), ())))
                parts[i, zz] = terms.astype(BF16).reshape(ny, p.own, p.cw)

            for e in range(1, ny):
                ry(i, e).start()

        @pl.when((i >= 1) & (i <= p.ns))
        def _():
            n = i - 1
            for e in range(1, ny):
                ry(n, e).wait_recv()

            @pl.loop(0, nz)
            def _(o):
                total = parts[n, o, y].astype(F32)
                for e in range(1, ny):
                    total += yb[n, e - 1, o].astype(F32)
                parts[n, o, y] = total.astype(BF16)
                pl.when(o == z)(lambda: add_stream(n, total))

        right = i - 1 - z

        @pl.when((right >= 0) & (right < p.ns))
        def _():
            for o in range(1, nz):

                @pl.when((o >= z) & (z > 0))
                def _(o=o):
                    rz_right(right, o).wait_recv()

                @pl.when((o > z) & (z > 0))
                def _(o=o):
                    parts[right, o, y] = (
                        parts[right, o, y].astype(F32) + lb[right, o - 1].astype(F32)
                    ).astype(BF16)

                pl.when(o > z)(lambda o=o: rz_right(right, o).start())
                pl.when(o == z)(lambda o=o: add_stream(right, lb[right, o - 1].astype(F32)))

        left = i - 1 - (nz - 1 - z)

        @pl.when((left >= 0) & (left < p.ns))
        def _():
            for o in range(nz - 1):

                @pl.when((o <= z) & (z < nz - 1))
                def _(o=o):
                    rz_left(left, o).wait_recv()

                @pl.when((o < z) & (z < nz - 1))
                def _(o=o):
                    parts[left, o, y] = (
                        parts[left, o, y].astype(F32) + rb[left, o].astype(F32)
                    ).astype(BF16)

                pl.when(o < z)(lambda o=o: rz_left(left, o).start())
                pl.when(o == z)(lambda o=o: add_stream(left, rb[left, o].astype(F32)))

        return 0

    lax.fori_loop(0, p.ns + nz, step, 0)
    out[...] = stream[...].astype(BF16)

    for e in range(1, nx):
        state_x(e).wait_send()
    for dist in range(1, nz):
        pl.when(z + dist < nz)(lambda dist=dist: state_z(dist).wait_send())

    @pl.loop(0, p.nj)
    def _(j):
        for m in range(3):
            for i in range(p.zc):
                first_hop(m, j, i).wait_send()

            @pl.when(duty)
            def _(m=m):
                for zz in range(nz):
                    for e in range(1, nx):
                        across(m, j, zz, e).wait_send()
                peer_all(m, j).wait_send()

    @pl.loop(0, p.ns)
    def _(n):
        for e in range(1, ny):
            ry(n, e).wait_send()
        for o in range(nz):
            if o:
                pl.when(o > z)(lambda o=o: rz_right(n, o).wait_send())
            if o < nz - 1:
                pl.when(o < z)(lambda o=o: rz_left(n, o).wait_send())


def solution(mesh):
    def per_device(*args):
        (residual, queries, keys, values, out_gate, in_gate, forget, extra, head_gain, out_w,
         ff_gain, gate_w, up_w, down_w) = args
        p = Plan(
            dict(mesh.shape),
            {
                "residual": residual.shape, "queries": queries.shape, "values": values.shape,
                "gates": in_gate.shape, "gate": gate_w.shape,
            },
        )
        vmem = pl.BlockSpec(memory_space=pltpu.VMEM)
        hbm = pl.BlockSpec(memory_space=pl.ANY)
        dma = pltpu.SemaphoreType.DMA
        held = jax.ShapeDtypeStruct((p.sp, p.rows, p.hid), BF16)
        nj, nz, nx, ny, ns = p.nj, p.nz, p.nx, p.ny, p.ns
        cols_used = p.d // p.cw
        cols8 = -(-2 * p.heads // 8) * 8
        scratch = [
            pltpu.VMEM((p.tok, cols8), F32),
            pltpu.VMEM((p.tok, p.vw), BF16),
            pltpu.VMEM((nx, p.state_rows, LANES), F32),
            pltpu.VMEM((nz, p.state_rows, LANES), F32),
            pltpu.VMEM((p.state_rows, LANES), F32),
            pltpu.VMEM((nz, ny, p.own, p.d), BF16),
            pltpu.VMEM((nz, 2, ny * p.own, p.hid), F32),
            pltpu.VMEM((2, p.sp * LANES, p.hid), BF16),
            pltpu.VMEM((ns, nz, ny, p.own, p.cw), BF16),
            pltpu.VMEM((ns, ny - 1, nz, p.own, p.cw), BF16),
            pltpu.VMEM((ns, nz - 1, p.own, p.cw), BF16),
            pltpu.VMEM((ns, nz - 1, p.own, p.cw), BF16),
            pltpu.VMEM((p.own, p.d), F32),
            pltpu.VMEM((cols_used, ny, p.own, p.cw), BF16),
            pltpu.VMEM((cols_used, ny - 1, p.own, p.cw), BF16),
            pltpu.VMEM((p.own, p.d), BF16),
            dma((3, nj, p.zc)), dma((3, nj, nz)),
            dma((3, nj, nz, nx - 1)), dma((3, nj, nz, nx - 1)),
            dma((3, nj)), dma((3, nj)),
            dma((nx - 1,)), dma((nx - 1,)),
            dma((nz - 1,)), dma((nz,)),
            dma((ny,)), dma((ny,)), dma((ny - 1,)), dma((ny - 1,)),
            dma((nz, GATHER_CUTS)), dma((nz, GATHER_CUTS)), dma((nz, GATHER_CUTS)),
            dma((nz, GATHER_CUTS, ny - 1)), dma((nz, GATHER_CUTS, ny - 1)),
            dma((ns, ny - 1)), dma((ns, ny - 1)),
            dma((ns, nz)), dma((ns, nz)), dma((ns, nz)), dma((ns, nz)),
            dma((3,)),
        ]
        result = pl.pallas_call(
            functools.partial(layer, p),
            out_shape=(
                jax.ShapeDtypeStruct((p.own, p.d), BF16), held, held, held,
            ),
            in_specs=[hbm] + [vmem] * 8 + [hbm, vmem] + [hbm] * 3,
            out_specs=(vmem, hbm, hbm, hbm),
            scratch_shapes=scratch,
            compiler_params=pltpu.CompilerParams(
                collective_id=0, has_side_effects=True, vmem_limit_bytes=67043328
            ),
            name="layer",
        )(
            residual, queries, keys, values, out_gate, in_gate, forget, extra,
            head_gain.reshape(1, -1), out_w, ff_gain.reshape(1, -1), gate_w, up_w, down_w,
        )
        return result[0]

    in_specs = (
        P("sp", None), P("sp", "tp"), P("sp", "tp"), P("sp", "tp"), P("sp", "tp"),
        P("tp", "sp"), P("tp", "sp"), P("tp", "sp"), P("tp"), P("tp", None), P(),
        P("sp", "tp"), P("sp", "tp"), P("sp", "tp"),
    )
    return jax.shard_map(
        per_device, mesh=mesh, in_specs=in_specs, out_specs=P(("sp", "tp"), None), check_vma=False
    )
```

profile of v0, /device:TPU:0, one launch (start us, length us, event | category | flops | bytes accessed | tf_op | source)
XLA Modules:
  0.0 454.3 jit_solution(7383702914849102276)
XLA Ops:
  0.0 1.3 reshape.6.refs_8_
  1.3 1.3 reshape.7.refs_10_
  2.6 449.4 %layer.1 = (bf16[128,4096]{1,0:T(8,128)(2,1)}, bf16[8,512,1408]{2,1,0:T(8,128)(2,1)}, bf16[8,512,1408]{2,1,0:T(8,128)(2,1)}, bf16[8,512,1408]{2,1,0:T(8,128)(2,1)}) custom-call(bf16[512,4096]{1,0:T(8,128)(2,1)} %refs_0_.1, bf16[512,256]{1,0:T(8,128)(2,1)} %refs_1_.1, bf16[512,256]{1,0:T(8,128)(2,1)} %refs_2_.1, bf16[512,512]{1,0:T(8,128)(2,1)} %refs_3_.1, ...), custom_call_target="tpu_custom_call" | custom-call | tf_op jit(solution)/shard_map/layer/pallas_call | solution.py:740
  452.0 2.3 copy.16
where the time goes:
time: 455 us; the launch traced here: 454 us
  Pallas kernels  449 us (99%)
  local copies, waits for them, and re-layouts  4.87 us (1%)
    pallas_call x1, Pallas kernels, per_device(): pl.pallas_call(functools.partial(layer, p), out_shape=(jax.ShapeDtypeStru...  449 us

commit v1 on v0

--- a/solution.py
+++ b/solution.py
@@ -13,7 +13,7 @@
 QUERY_ROWS = 256
 TOKEN_ROWS = 256
 GATHER_CUTS = 2
-EARLY_GROUPS = 3
+EARLY_GROUPS = 2
 
 
 class Plan:
@@ -143,26 +143,47 @@
 
     def send_group(ms, j):
         for i in range(p.zc):
-            for m in ms:
-                first_hop(m, j, i).start()
-
-    def each_z(fn):
-        fn(z)
+
+            @pl.when(c * p.zc + i != z)
+            def _(i=i):
+                for m in ms:
+                    first_hop(m, j, i).start()
+
+    def send_own():
+        for i in range(p.zc):
+
+            @pl.when(c * p.zc + i == z)
+            def _(i=i):
+                for m in range(3):
+                    for j in range(p.nj):
+                        first_hop(m, j, i).start()
+
+    def each_other(fn):
         for dist in range(1, nz):
             pl.when(z - dist >= 0)(functools.partial(fn, z - dist))
             pl.when(z + dist < nz)(functools.partial(fn, z + dist))
 
+    def each_z(fn):
+        fn(z)
+        each_other(fn)
+
+    def pass_on(ms, j, zs_):
+        for m in ms:
+            first_recv(m, j, zs_).wait_recv()
+            for e in range(1, nx):
+                across(m, j, zs_, e).start()
+            to_peer(m, j, zs_ * nx + x).start()
+
     def relay(ms, j):
         @pl.when(duty)
         def _():
-            def one(zs_):
-                for m in ms:
-                    first_recv(m, j, zs_).wait_recv()
-                    for e in range(1, nx):
-                        across(m, j, zs_, e).start()
-                    to_peer(m, j, zs_ * nx + x).start()
-
-            each_z(one)
+            each_other(functools.partial(pass_on, ms, j))
+
+    def relay_own(ms):
+        @pl.when(duty)
+        def _():
+            for j in range(p.nj):
+                pass_on(ms, j, z)
 
     def settle(ms, j):
         @pl.when(duty)
@@ -180,7 +201,8 @@
             for m in ms:
                 peer_all(m, j).wait_recv()
 
-    send_group((0, 1), 0)
+    send_group((0,), 0)
+    send_own()
     fetch_res = pltpu.make_async_copy(
         residual.at[pl.ds(pl.multiple_of(tp_i * p.own, p.own), p.own), :], res, local.at[2]
     )
@@ -290,8 +312,10 @@
 
     for dist in range(1, nz):
         pl.when(z + dist < nz)(lambda dist=dist: state_z(dist).start())
+    send_group((1,), 0)
     for j in range(1, min(EARLY_GROUPS, p.nj)):
         send_group((0, 1), j)
+    relay_own((0, 1))
 
     reset(carry)
     for i in range(nz - 1):
@@ -347,8 +371,6 @@
             gates = jax.nn.sigmoid(out_gate[r0:r1, span].astype(F32))
             gated[r0:r1, span] = (cell * lax.rsqrt(square + 1e-06) * gain * gates).astype(BF16)
 
-    relay((0, 1), 0)
-
     pieces = p.d // p.wc
 
     def fetch_w(n):
@@ -383,7 +405,6 @@
 
     for yy in range(ny):
         at_peer(yy).start()
-    relay((0, 1), 1)
 
     def at_y(e):
         b = mod(y, e, ny) * nc + c
@@ -410,7 +431,7 @@
             res[:, cols].astype(F32)
             + parts[n, b // ny, lax.rem(b, ny)].astype(F32) + cr[n, y].astype(F32)
         )
-    settle((0, 1), 0)
+    relay((0, 1), 0)
     for e in range(1, ny):
         at_y(e).wait_recv()
         for n in range(cols_used):
@@ -450,6 +471,9 @@
         pl.when(z >= 1)(lambda s=s: go_left(z, s).start())
         for e in range(1, ny):
             go_y(z, s, e).start()
+    relay_own((2,))
+    for j in range(1, min(EARLY_GROUPS, p.nj)):
+        relay((0, 1), j)
     for dist in range(1, nz):
         for s in range(GATHER_CUTS):
 
@@ -467,14 +491,14 @@
                 for e in range(1, ny):
                     go_y(z + dist, s, e).start()
 
-        if dist == 1:
-            relay((0, 1), 2 % p.nj) if p.nj > 2 else None
     for j in range(min(EARLY_GROUPS, p.nj), p.nj):
         send_group((0, 1), j)
     for j in range(p.nj):
         send_group((2,), j)
-    for j in range(1, min(3, p.nj)):
+    for j in range(min(EARLY_GROUPS, p.nj)):
         settle((0, 1), j)
+    if p.nj > EARLY_GROUPS:
+        relay((0, 1), EARLY_GROUPS)
     for zz in range(nz):
         for s in range(GATHER_CUTS):
             for e in range(1, ny):
@@ -506,8 +530,9 @@
         return pltpu.make_async_copy(slab.at[m], slab.at[m], local.at[m])
 
     for j in range(p.nj):
-        if j >= 3:
-            relay((0, 1), j)
+        if j >= EARLY_GROUPS:
+            if j + 1 < p.nj:
+                relay((0, 1), j + 1)
             settle((0, 1), j)
         for m in range(2):
             for copy in load_slab(m, j):
@@ -533,6 +558,8 @@
                 else:
                     acc[zz, m] += more
 
+    relay((2,), 0)
+
     @pl.loop(0, nz)
     def _(zz):
         hidden = jax.nn.silu(acc[zz, 0]) * acc[zz, 1]
@@ -587,7 +614,6 @@
 
             @pl.when(lax.rem(i, p.halves) == 0)
             def _():
-                relay((2,), j)
                 settle((2,), j)
 
             for copy in load_down(i):
@@ -603,6 +629,10 @@
 
             for e in range(1, ny):
                 ry(i, e).start()
+
+            @pl.when((lax.rem(i, p.halves) == 0) & (j + 1 < p.nj))
+            def _():
+                relay((2,), j + 1)
 
         @pl.when((i >= 1) & (i <= p.ns))
         def _():
@@ -622,7 +652,7 @@
 
         @pl.when((right >= 0) & (right < p.ns))
         def _():
-            for o in range(1, nz):
+            for o in range(nz - 1, 0, -1):
 
                 @pl.when((o >= z) & (z > 0))
                 def _(o=o):

time: 455 us -> 370 us (0.81)
  Pallas kernels: 449 us -> 364 us
    pallas_call x1, Pallas kernels: 449 us -> 364 us  [per_device(): pl.pallas_call(functools.partial(layer, p), out_shape=(jax.ShapeDtypeStru...]
where the time goes in v1:
time: 370 us; the launch traced here: 369 us
  Pallas kernels  364 us (98%)
  local copies, waits for them, and re-layouts  4.87 us (1%)
    pallas_call x1, Pallas kernels, per_device(): pl.pallas_call(functools.partial(layer, p), out_shape=(jax.ShapeDtypeStru...  364 us

profile of v1, /device:TPU:0, one launch (start us, length us, event | category | flops | bytes accessed | tf_op | source)
XLA Modules:
  0.0 369.2 jit_solution(4512647335721481423)
XLA Ops:
  0.0 1.3 reshape.6.refs_8_
  1.3 1.3 reshape.7.refs_10_
  2.6 364.3 %layer.1 = (bf16[128,4096]{1,0:T(8,128)(2,1)}, bf16[8,512,1408]{2,1,0:T(8,128)(2,1)}, bf16[8,512,1408]{2,1,0:T(8,128)(2,1)}, bf16[8,512,1408]{2,1,0:T(8,128)(2,1)}) custom-call(bf16[512,4096]{1,0:T(8,128)(2,1)} %refs_0_.1, bf16[512,256]{1,0:T(8,128)(2,1)} %refs_1_.1, bf16[512,256]{1,0:T(8,128)(2,1)} %refs_2_.1, bf16[512,512]{1,0:T(8,128)(2,1)} %refs_3_.1, ...), custom_call_target="tpu_custom_call" | custom-call | tf_op jit(solution)/shard_map/layer/pallas_call | solution.py:770
  366.9 2.3 copy.16

commit v2 on v1

--- a/solution.py
+++ b/solution.py
@@ -533,6 +533,8 @@
         if j >= EARLY_GROUPS:
             if j + 1 < p.nj:
                 relay((0, 1), j + 1)
+            else:
+                relay((2,), 0)
             settle((0, 1), j)
         for m in range(2):
             for copy in load_slab(m, j):
@@ -558,7 +560,10 @@
                 else:
                     acc[zz, m] += more
 
-    relay((2,), 0)
+    if p.nj <= EARLY_GROUPS:
+        relay((2,), 0)
+    if p.nj > 1:
+        relay((2,), 1)
 
     @pl.loop(0, nz)
     def _(zz):
@@ -630,9 +635,9 @@
             for e in range(1, ny):
                 ry(i, e).start()
 
-            @pl.when((lax.rem(i, p.halves) == 0) & (j + 1 < p.nj))
+            @pl.when((lax.rem(i, p.halves) == 0) & (j + 2 < p.nj))
             def _():
-                relay((2,), j + 1)
+                relay((2,), j + 2)
 
         @pl.when((i >= 1) & (i <= p.ns))
         def _():

time: 370 us -> 363 us (0.981)
  Pallas kernels: 364 us -> 355 us
    pallas_call x1, Pallas kernels: 364 us -> 355 us  [per_device(): pl.pallas_call(functools.partial(layer, p), out_shape=(jax.ShapeDtypeStru...]
where the time goes in v2:
time: 363 us; the launch traced here: 360 us
  Pallas kernels  355 us (98%)
  local copies, waits for them, and re-layouts  4.87 us (1%)
    pallas_call x1, Pallas kernels, per_device(): pl.pallas_call(functools.partial(layer, p), out_shape=(jax.ShapeDtypeStru...  355 us

profile of v2, /device:TPU:0, one launch (start us, length us, event | category | flops | bytes accessed | tf_op | source)
XLA Modules:
  0.0 359.8 jit_solution(14355798470828169186)
XLA Ops:
  0.0 1.3 reshape.6.refs_8_
  1.3 1.3 reshape.7.refs_10_
  2.6 354.9 %layer.1 = (bf16[128,4096]{1,0:T(8,128)(2,1)}, bf16[8,512,1408]{2,1,0:T(8,128)(2,1)}, bf16[8,512,1408]{2,1,0:T(8,128)(2,1)}, bf16[8,512,1408]{2,1,0:T(8,128)(2,1)}) custom-call(bf16[512,4096]{1,0:T(8,128)(2,1)} %refs_0_.1, bf16[512,256]{1,0:T(8,128)(2,1)} %refs_1_.1, bf16[512,256]{1,0:T(8,128)(2,1)} %refs_2_.1, bf16[512,512]{1,0:T(8,128)(2,1)} %refs_3_.1, ...), custom_call_target="tpu_custom_call" | custom-call | tf_op jit(solution)/shard_map/layer/pallas_call | solution.py:775
  357.5 2.3 copy.16

commit v3 on v2

--- a/solution.py
+++ b/solution.py
@@ -158,8 +158,8 @@
                     for j in range(p.nj):
                         first_hop(m, j, i).start()
 
-    def each_other(fn):
-        for dist in range(1, nz):
+    def each_other(fn, least=1, most=None):
+        for dist in range(least, most or nz):
             pl.when(z - dist >= 0)(functools.partial(fn, z - dist))
             pl.when(z + dist < nz)(functools.partial(fn, z + dist))
 
@@ -174,10 +174,16 @@
                 across(m, j, zs_, e).start()
             to_peer(m, j, zs_ * nx + x).start()
 
-    def relay(ms, j):
+    def relay(ms, j, least=1, most=None):
         @pl.when(duty)
         def _():
-            each_other(functools.partial(pass_on, ms, j))
+            each_other(functools.partial(pass_on, ms, j), least, most)
+
+    def relay_near(ms, j):
+        relay(ms, j, 1, 2)
+
+    def relay_far(ms, j):
+        relay(ms, j, 2)
 
     def relay_own(ms):
         @pl.when(duty)
@@ -531,11 +537,11 @@
 
     for j in range(p.nj):
         if j >= EARLY_GROUPS:
+            coming = ((0, 1), j + 1) if j + 1 < p.nj else ((2,), 0)
+            relay_near(*coming)
+            settle((0, 1), j)
             if j + 1 < p.nj:
-                relay((0, 1), j + 1)
-            else:
-                relay((2,), 0)
-            settle((0, 1), j)
+                relay_far(*coming)
         for m in range(2):
             for copy in load_slab(m, j):
                 copy.start()
@@ -562,6 +568,8 @@
 
     if p.nj <= EARLY_GROUPS:
         relay((2,), 0)
+    else:
+        relay_far((2,), 0)
     if p.nj > 1:
         relay((2,), 1)
 

time: 363 us -> 367 us (1.011)
  Pallas kernels: 355 us -> 361 us
    pallas_call x1, Pallas kernels: 355 us -> 361 us  [per_device(): pl.pallas_call(functools.partial(layer, p), out_shape=(jax.ShapeDtypeStru...]
where the time goes in v3:
time: 367 us; the launch traced here: 366 us
  Pallas kernels  361 us (98%)
  local copies, waits for them, and re-layouts  4.87 us (1%)
    pallas_call x1, Pallas kernels, per_device(): pl.pallas_call(functools.partial(layer, p), out_shape=(jax.ShapeDtypeStru...  361 us

profile of v3, /device:TPU:0, one launch (start us, length us, event | category | flops | bytes accessed | tf_op | source)
XLA Modules:
  0.0 366.1 jit_solution(10588463767063827723)
XLA Ops:
  0.0 1.3 reshape.6.refs_8_
  1.3 1.3 reshape.7.refs_10_
  2.6 361.2 %layer.1 = (bf16[128,4096]{1,0:T(8,128)(2,1)}, bf16[8,512,1408]{2,1,0:T(8,128)(2,1)}, bf16[8,512,1408]{2,1,0:T(8,128)(2,1)}, bf16[8,512,1408]{2,1,0:T(8,128)(2,1)}) custom-call(bf16[512,4096]{1,0:T(8,128)(2,1)} %refs_0_.1, bf16[512,256]{1,0:T(8,128)(2,1)} %refs_1_.1, bf16[512,256]{1,0:T(8,128)(2,1)} %refs_2_.1, bf16[512,512]{1,0:T(8,128)(2,1)} %refs_3_.1, ...), custom_call_target="tpu_custom_call" | custom-call | tf_op jit(solution)/shard_map/layer/pallas_call | solution.py:783
  363.8 2.3 copy.16
